TPU v7x, 128 devices: a whole 4x4x4 slice. The times are simulated.
128 devices in a mesh: fs: 16 (over z, x), tp: 8 (over y, core).
Axes of the slice: x: 4, y: 4, z: 4, core: 2. Of those that a mesh axis runs over, the one named last changes fastest.
Arguments:
- normed_input: bfloat16 [32768, 2048], P('fs'), may hold values from -6 to 6
- forget_cot: bfloat16 [32768, 2048], P('fs', 'tp'), may hold values from -6 to 6
- value_cot: bfloat16 [32768, 2048], P('fs', 'tp'), may hold values from -6 to 6
- gated_output: bfloat16 [32768, 2048], P('fs', 'tp'), may hold values from -6 to 6
- output_cot: bfloat16 [32768, 2048], P('fs'), may hold values from -6 to 6
- forget_weight: float32 [2048, 2048], P('fs', 'tp'), may hold values from -0.125 to 0.125
- value_weight: float32 [2048, 2048], P('fs', 'tp'), may hold values from -0.125 to 0.125
- out_weight: float32 [2048, 2048], P('tp', 'fs'), may hold values from -0.125 to 0.125
- bases: bfloat16 [3, 2048, 256], replicated, may hold values from -0.125 to 0.125
- first_moment: float32 [256, 3, 2048], P('fs', None, 'tp'), may hold values from -4 to 4
- second_moment: float32 [256, 3, 2048], P('fs', None, 'tp'), may hold values from 0.25 to 4
Outputs:
- new_forget: float32 [2048, 2048], P('fs', 'tp')
- new_value: float32 [2048, 2048], P('fs', 'tp')
- new_out: float32 [2048, 2048], P('tp', 'fs')
- copy_forget: bfloat16 [2048, 2048], P(None, 'tp')
- copy_value: bfloat16 [2048, 2048], P(None, 'tp')
- copy_out: bfloat16 [2048, 2048], P('tp')
- moment_one: float32 [256, 3, 2048], P('fs', None, 'tp')
- moment_two: float32 [256, 3, 2048], P('fs', None, 'tp')
- step_forget: float32 [2048, 2048], P('fs', 'tp')
- step_value: float32 [2048, 2048], P('fs', 'tp')
- step_out: float32 [2048, 2048], P('tp', 'fs')
All inputs are finite; a program needn't handle non-finite values.
Results may differ from a plain program's by a relative error of at most 0.0045.
Values may be sent and summed in bfloat16 or wider, within the bound.
No kernel may reach another device: no remote copies, remote signals or barrier semaphores. Data moves between devices by JAX's collectives and lax.ppermute only.
A program may use at most 128 MiB of HBM per device.

v0:
```python
import functools
import jax
import jax.numpy as jnp
from jax import lax
from jax.sharding import Mesh
from jax.sharding import PartitionSpec as P

FS = ("fs_0", "fs_1")
FS_TP = ("fs_0", "fs_1", "tp_0", "tp_1")
TP = ("tp_0", "tp_1")


def in_blocks(value, dim, count):
    before, after = (value.shape[:dim], value.shape[dim + 1 :])
    return jnp.moveaxis(value.reshape(*before, count, -1, *after), dim, 0)


def sum_at_owner(value, axis, dim):
    pieces = in_blocks(value, dim, lax.axis_size(axis))
    arrived = lax.all_to_all(pieces, axis, split_axis=0, concat_axis=0, tiled=True)
    return arrived.astype(jnp.float32).sum(axis=0)


def joined_along(pieces, dim):
    dims = list(pieces.shape[1:])
    dims[dim] *= pieces.shape[0]
    return jnp.moveaxis(pieces, 0, dim).reshape(dims)


def sent_to_all(value, axis):
    copies = jnp.broadcast_to(value, (lax.axis_size(axis), *value.shape))
    return lax.all_to_all(copies, axis, split_axis=0, concat_axis=0, tiled=True)


def gather_directly(value, axis, dim):
    return joined_along(sent_to_all(value, axis), dim)


def over_axes(value, axes):
    return functools.reduce(lax.psum, axes, value)


def gather_turned(arrays, axis, dims):
    turned = [jnp.moveaxis(a, dim, 0) for a, dim in zip(arrays, dims)]
    both = jnp.concatenate([t.reshape(len(t), -1) for t in turned], axis=1)
    result, at, finished = (lax.all_gather(both, axis, axis=0, tiled=True), 0, [])
    for t, dim in zip(turned, dims):
        piece = result[:, at : at + t[0].size].reshape(-1, *t.shape[1:])
        finished.append(jnp.moveaxis(piece, 0, dim))
        at += t[0].size
    return tuple(finished)


def split_parts(values):
    high = lax.optimization_barrier(values.astype(jnp.bfloat16))
    low = (values - high.astype(jnp.float32)).astype(jnp.bfloat16)
    return (high, low)


def on_device(
    normed_input,
    forget_cot,
    value_cot,
    gated_output,
    output_cot,
    forget_weight,
    value_weight,
    out_weight,
    bases,
    first_moment,
    second_moment,
):
    rows = forget_weight.shape[0]
    rank_rows = first_moment.shape[0]
    columns = forget_weight.shape[1]
    offset = lax.axis_index(FS) * rows
    factor = float(normed_input.shape[0] * lax.axis_size(FS)) ** (-0.5)
    my_bases = lax.dynamic_slice_in_dim(bases, offset, rows, 1)
    reduced = jnp.stack(
        [
            jnp.dot(normed_input, bases[0], preferred_element_type=jnp.float32),
            jnp.dot(normed_input, bases[1], preferred_element_type=jnp.float32),
            jnp.dot(output_cot, bases[2], preferred_element_type=jnp.float32),
        ],
        axis=1,
    )
    reduced_high, reduced_low = split_parts(reduced)
    paired = jnp.stack([forget_cot, value_cot, gated_output], axis=1)
    upper = jnp.einsum("tkr,tkc->rkc", reduced_high, paired, preferred_element_type=jnp.float32)
    lower = jnp.einsum("tkr,tkc->rkc", reduced_low, paired, preferred_element_type=jnp.float32)
    projected = sum_at_owner(((upper + lower) * factor).astype(jnp.bfloat16), FS, 0)
    moment_one = 0.9 * first_moment + 0.1 * projected
    moment_two = 0.9 * second_moment + 0.1 * projected * projected
    direction = moment_one / (jnp.sqrt(moment_two) + 1e-08)
    piece_high, piece_low = split_parts(gather_directly(direction, FS, 0))
    upper = jnp.einsum("kdr,rkc->dkc", my_bases, piece_high, preferred_element_type=jnp.float32)
    lower = jnp.einsum("kdr,rkc->dkc", my_bases, piece_low, preferred_element_type=jnp.float32)
    full = upper + lower
    totals = over_axes(jnp.sum(direction * direction, axis=(0, 2)), FS_TP)
    entries = rank_rows * lax.axis_size(FS) * columns * lax.axis_size(TP)
    scale = lax.rsqrt(totals / entries + 1.0)
    full = full * scale[None, :, None]
    step_forget = full[:, 0, :]
    step_value = full[:, 1, :]
    step_out = full[:, 2, :].T
    new_forget = forget_weight - 0.01 * step_forget
    new_value = value_weight - 0.01 * step_value
    new_out = out_weight - 0.01 * step_out
    copy_forget, copy_value, copy_out = gather_turned(
        (
            new_forget.astype(jnp.bfloat16),
            new_value.astype(jnp.bfloat16),
            new_out.astype(jnp.bfloat16),
        ),
        FS,
        (0, 0, 1),
    )
    return (
        new_forget,
        new_value,
        new_out,
        copy_forget,
        copy_value,
        copy_out,
        moment_one,
        moment_two,
        step_forget,
        step_value,
        step_out,
    )


def solution(mesh):
    torus = Mesh(mesh.devices.reshape(4, 4, 4, 2), ("fs_0", "fs_1", "tp_0", "tp_1"))
    placed = (
        P(FS, None),
        P(FS, TP),
        P(FS, TP),
        P(FS, TP),
        P(FS, None),
        P(FS, TP),
        P(FS, TP),
        P(TP, FS),
        P(),
        P(FS, None, TP),
        P(FS, None, TP),
    )
    return jax.shard_map(
        on_device,
        mesh=torus,
        in_specs=placed,
        out_specs=(
            P(FS, TP),
            P(FS, TP),
            P(TP, FS),
            P(None, TP),
            P(None, TP),
            P(TP, None),
            P(FS, None, TP),
            P(FS, None, TP),
            P(FS, TP),
            P(FS, TP),
            P(TP, FS),
        ),
        check_vma=False,
    )
```

profile of v0, /device:TPU:0, one launch (start us, length us, event | category | flops | bytes accessed | tf_op | source)
XLA Modules:
  0.0 149.7 jit_solution(3815490610961850263)
XLA Ops:
  7.2 6.1 %convolution_bitcast_fusion.1 = f32[2048,1,256]{2,0,1:T(8,128)S(1)} fusion(bf16[2048,2048]{1,0:T(8,128)(2,1)} %param.11, bf16[3,2048,256]{2,1,0:T(8,128)(2,1)} %param.19), kind=kOutput, calls=%fused_computation.6 | convolution fusion | flops 2147483648 | bytes 11534336 | tf_op jit(solution)/shard_map/dot_general | solution.py:82
  13.3 0.9 copy-done.6
  14.2 2.5 %convolution_bitcast_fusion.2 = f32[2048,1,256]{2,0,1:T(8,128)S(1)} fusion(bf16[2048,2048]{1,0:T(8,128)(2,1)S(1)} %copy-done.6, bf16[3,2048,256]{2,1,0:T(8,128)(2,1)S(1)} %copy-done.3), kind=kOutput, calls=%fused_computation.7 | convolution fusion | flops 2147483648 | bytes 11534336 | tf_op jit(solution)/shard_map/dot_general | solution.py:81
  16.8 2.4 %convolution_bitcast_fusion = f32[2048,1,256]{2,0,1:T(8,128)S(1)} fusion(bf16[2048,2048]{1,0:T(8,128)(2,1)S(1)} %bitcast.55, bf16[3,2048,256]{2,1,0:T(8,128)(2,1)S(1)} %copy-done.3), kind=kOutput, calls=%fused_computation.5 | convolution fusion | flops 2147483648 | bytes 11534336 | tf_op jit(solution)/shard_map/dot_general | solution.py:83
  21.1 1.4 fusion.1
  22.5 1.3 fusion.5
  23.9 18.0 %all_to_all.10 = bf16[16,16,3,256]{3,1,2,0:T(8,128)(2,1)S(1)} all-to-all(bf16[16,16,3,256]{3,1,2,0:T(8,128)(2,1)S(1)} %copy.47), channel_id=1, replica_groups=mesh['fs_0'=4,'fs_1'=4,'tp_0'=4,'tp_1'=2] {'fs_0','fs_1'}, dimensions={0} | all-to-all | bytes 786432 | tf_op jit(solution)/shard_map/all_to_all | solution.py:20
  42.6 1.0 broadcast_in_dim.4
  43.6 3.6 %all-to-all-start.1 = ((f32[16,16,3,256]{3,1,2,0:T(8,128)}), f32[16,16,3,256]{3,1,2,0:T(8,128)S(1)}, u32[]{:S(2)}, u32[]{:S(2)}) async-start(f32[16,16,3,256]{3,1,2,0:T(8,128)} %broadcast_in_dim.4), calls=%async_computation.1 | async-start | bytes 1572864 | tf_op jit(solution)/shard_map/all_to_all | solution.py:32
  47.3 14.0 %psum.28 = f32[3]{0:T(128)S(1)} all-reduce(f32[3]{0:T(128)S(1)} %get-tuple-element.51), channel_id=1, replica_groups=mesh['fs_0'=4,'fs_1'=4,'tp_0'=4,'tp_1'=2] {'fs_0'}, use_global_device_ids=true, to_apply=%region_2.0 | all-reduce | flops 3 | bytes 24 | tf_op jit(solution)/shard_map/psum | solution.py:40
  61.4 10.5 %psum.29 = f32[3]{0:T(128)S(1)} all-reduce(f32[3]{0:T(128)S(1)} %psum.28), channel_id=1, replica_groups=mesh['fs_0'=4,'fs_1'=4,'tp_0'=4,'tp_1'=2] {'fs_1'}, use_global_device_ids=true, to_apply=%region_3.0 | all-reduce | flops 3 | bytes 24 | tf_op jit(solution)/shard_map/psum | solution.py:40
  72.0 10.7 %psum.30 = f32[3]{0:T(128)S(1)} all-reduce(f32[3]{0:T(128)S(1)} %psum.29), channel_id=1, replica_groups=mesh['fs_0'=4,'fs_1'=4,'tp_0'=4,'tp_1'=2] {'tp_0'}, use_global_device_ids=true, to_apply=%region_4.0 | all-reduce | flops 3 | bytes 24 | tf_op jit(solution)/shard_map/psum | solution.py:40
  82.7 2.5 %psum.31 = f32[3]{0:T(128)S(1)} all-reduce(f32[3]{0:T(128)S(1)} %psum.30), channel_id=1, replica_groups=mesh['fs_0'=4,'fs_1'=4,'tp_0'=4,'tp_1'=2] {'tp_1'}, use_global_device_ids=true, to_apply=%region_5.0 | all-reduce | flops 3 | bytes 24 | tf_op jit(solution)/shard_map/psum | solution.py:40
  85.4 1.2 fusion.16
  86.7 1.2 fusion.7
  87.9 0.7 convert_bitcast_fusion
  89.4 0.8 copy.53
  90.2 0.8 copy.54
  91.0 0.8 copy.57
  91.7 0.8 copy.58
  92.5 44.7 %all-gather.2.cloned.1.call-done = bf16[2048,768]{0,1:T(8,128)(2,1)} async-done(((bf16[128,768]{0,1:T(8,128)(2,1)}), bf16[2048,768]{0,1:T(8,128)(2,1)}) %all-gather.2.cloned.1.call-update) | async-done | bytes 3145744 | tf_op jit(solution)/shard_map/all_gather | solution.py:46
  137.2 3.1 %slice_bitcast_fusion = (bf16[256,2048]{1,0:T(8,128)(2,1)}, bf16[2048,256]{0,1:T(8,128)(2,1)S(1)}, bf16[2048,256]{0,1:T(8,128)(2,1)S(1)}) fusion(bf16[2048,768]{0,1:T(8,128)(2,1)} %all-gather.2.cloned.1.call-done), kind=kLoop, calls=%fused_computation.15 | loop fusion | bytes 6291456 | tf_op jit(solution)/shard_map/transpose | solution.py:49
  140.3 1.3 copy.55
  141.6 1.3 copy.56
  (40 shorter events, 4.0 us)
Async XLA Ops:
  7.2 6.2 %copy-start.3 = (bf16[3,2048,256]{2,1,0:T(8,128)(2,1)S(1)}, bf16[3,2048,256]{2,1,0:T(8,128)(2,1)}, u32[]{:S(2)}) copy-start(bf16[3,2048,256]{2,1,0:T(8,128)(2,1)} %param.19) | copy-start | bytes 9437188
  7.2 7.0 %copy-start.6 = (bf16[2048,2048]{1,0:T(8,128)(2,1)S(1)}, bf16[2048,2048]{1,0:T(8,128)(2,1)}, u32[]{:S(2)}) copy-start(bf16[2048,2048]{1,0:T(8,128)(2,1)} %param.11) | copy-start | bytes 25165828
  7.2 9.5 %slice-start = ((s8[8388608]{0:T(1024)(128)(4,1)}), s8[4194304]{0:T(1024)(128)(4,1)S(1)}, s32[]{:S(2)}) async-start(s8[8388608]{0:T(1024)(128)(4,1)} %bitcast.54), calls=%async_computation.3 | async-start | bytes 8388608
  14.2 2.6 %slice-start.1 = ((s8[8388608]{0:T(1024)(128)(4,1)}), s8[4194304]{0:T(1024)(128)(4,1)S(1)}, s32[]{:S(2)}) async-start(s8[8388608]{0:T(1024)(128)(4,1)} %bitcast.54), calls=%async_computation.4 | async-start | bytes 8388608
  19.2 1.2 copy-start.7
  19.2 1.5 %copy-start.8 = (bf16[2048,256]{1,0:T(8,128)(2,1)S(1)}, bf16[2048,256]{1,0:T(8,128)(2,1)}, u32[]{:S(2)}) copy-start(bf16[2048,256]{1,0:T(8,128)(2,1)} %param.13) | copy-start | bytes 3145732
  19.2 1.8 %copy-start.9 = (bf16[2048,256]{1,0:T(8,128)(2,1)S(1)}, bf16[2048,256]{1,0:T(8,128)(2,1)}, u32[]{:S(2)}) copy-start(bf16[2048,256]{1,0:T(8,128)(2,1)} %param.12) | copy-start | bytes 3145732
  22.5 19.5 %copy-start.4 = (f32[16,3,256]{2,0,1:T(8,128)S(1)}, f32[16,3,256]{2,0,1:T(8,128)}, u32[]{:S(2)}) copy-start(f32[16,3,256]{2,0,1:T(8,128)} %param.21) | copy-start | bytes 147460
  22.5 19.5 %copy-start.5 = (f32[16,3,256]{2,0,1:T(8,128)S(1)}, f32[16,3,256]{2,0,1:T(8,128)}, u32[]{:S(2)}) copy-start(f32[16,3,256]{2,0,1:T(8,128)} %param.20) | copy-start | bytes 147460
  23.8 37.5 %copy-start = (f32[128,256]{1,0:T(8,128)S(1)}, f32[128,256]{1,0:T(8,128)}, u32[]{:S(2)}) copy-start(f32[128,256]{1,0:T(8,128)} %param.16) | copy-start | bytes 393220
  23.8 48.1 %copy-start.1 = (f32[128,256]{1,0:T(8,128)S(1)}, f32[128,256]{1,0:T(8,128)}, u32[]{:S(2)}) copy-start(f32[128,256]{1,0:T(8,128)} %param.17) | copy-start | bytes 393220
  43.6 41.6 %all-to-all-start.1 = ((f32[16,16,3,256]{3,1,2,0:T(8,128)}), f32[16,16,3,256]{3,1,2,0:T(8,128)S(1)}, u32[]{:S(2)}, u32[]{:S(2)}) async-start(f32[16,16,3,256]{3,1,2,0:T(8,128)} %broadcast_in_dim.4), calls=%async_computation.1 | async-start | bytes 1572864 | tf_op jit(solution)/shard_map/all_to_all | solution.py:32
  47.2 90.0 %all-gather.2.cloned.1.call-start = ((), (), s32[]{:S(2)}) async-start(), calls=%async_computation.2 | async-start | bytes 3342336 | tf_op jit(solution)/shard_map/all_gather | solution.py:46
  85.2 2.7 %copy-start.2 = (f32[256,128]{1,0:T(8,128)S(1)}, f32[256,128]{1,0:T(8,128)}, u32[]{:S(2)}) copy-start(f32[256,128]{1,0:T(8,128)} %param.18) | copy-start | bytes 393220
Sparse Core Ops, SparseCore 0:
  89.5 47.5 all-gather.1
where the time goes:
time: 150 us
  blocking collectives  55.7 us (37%)
  waiting for transfers between devices  44.7 us (30%)
  matrix products  16.1 us (11%)
  between operations  14.3 us (10%)
  local copies, waits for them, and re-layouts  12.2 us (8%)
  starting transfers between devices  3.66 us (2%)
  other arithmetic  2.94 us (2%)
    all_gather x1, waiting for transfers between devices, gather_turned(): lax.all_gather(both, axis, axis=0, tiled=True)  44.7 us
    psum x4, blocking collectives, over_axes(): return functools.reduce(lax.psum, axes, value)  37.7 us
    all_to_all x1, blocking collectives, sum_at_owner(): lax.all_to_all(pieces, axis, split_axis=0, concat_axis=0, tiled=True)  18 us
    unnamed x32, local copies, waits for them, and re-layouts  8.06 us
    dot_general x1, matrix products, on_device(): jnp.dot(normed_input, bases[1], preferred_element_type=jnp.float32)  6.11 us
    all_to_all x1, starting transfers between devices, sent_to_all(): return lax.all_to_all(copies, axis, split_axis=0, concat_axis=0, tiled=True)  3.61 us
    transpose x1, local copies, waits for them, and re-layouts, gather_turned(): finished.append(jnp.moveaxis(piece, 0, dim))  3.11 us
  transfers between devices with their start and end apart: 2, of which 1 were waited for; matrix products, arithmetic and copies ran while one was open for 2% of the time, Pallas kernels for 0%

commit v1 on v0

--- a/solution.py
+++ b/solution.py
@@ -43,7 +43,13 @@
 def gather_turned(arrays, axis, dims):
     turned = [jnp.moveaxis(a, dim, 0) for a, dim in zip(arrays, dims)]
     both = jnp.concatenate([t.reshape(len(t), -1) for t in turned], axis=1)
-    result, at, finished = (lax.all_gather(both, axis, axis=0, tiled=True), 0, [])
+    result, at, finished = (
+        jnp.concatenate(
+            lax.all_to_all(jnp.stack([both] * lax.axis_size(axis)), axis, 0, 0), axis=0
+        ),
+        0,
+        [],
+    )
     for t, dim in zip(turned, dims):
         piece = result[:, at : at + t[0].size].reshape(-1, *t.shape[1:])
         finished.append(jnp.moveaxis(piece, 0, dim))

time: 150 us -> 146 us (0.973)
  between operations: 14.3 us -> 0.91 us
  local copies, waits for them, and re-layouts: 12.2 us -> 20.7 us
  starting transfers between devices: 3.66 us -> 7.36 us
  waiting for transfers between devices: 44.7 us -> 41.7 us
    all_gather x1 -> x0, waiting for transfers between devices: 44.7 us -> none  [gather_turned(): lax.all_gather(both, axis, axis=0, tiled=True)]
    all_to_all x0 -> x1, waiting for transfers between devices: none -> 41.7 us  [gather_turned(): lax.all_to_all(jnp.stack([both] * lax.axis_size(axis)), axis, 0, 0)]
    all_to_all x0 -> x1, starting transfers between devices: none -> 3.74 us  [gather_turned(): lax.all_to_all(jnp.stack([both] * lax.axis_size(axis)), axis, 0, 0)]
    all_to_all x0 -> x1, local copies, waits for them, and re-layouts: none -> 2.79 us  [gather_turned(): lax.all_to_all(jnp.stack([both] * lax.axis_size(axis)), axis, 0, 0)]
    unnamed x32 -> x31, local copies, waits for them, and re-layouts: 8.06 us -> 10.5 us
    another operation x0 -> x1, local copies, waits for them, and re-layouts: none -> 2.26 us  [gather_turned(): jnp.stack([both] * lax.axis_size(axis))]
  transfers between devices with their start and end apart: 2 -> 2, of which waited for: 1 -> 1; matrix products, arithmetic and copies ran while one was open for 2% -> 5% of each run, Pallas kernels for 0% -> 0%
where the time goes in v1:
time: 146 us
  blocking collectives  56 us (38%)
  waiting for transfers between devices  41.7 us (29%)
  local copies, waits for them, and re-layouts  20.7 us (14%)
  matrix products  16.1 us (11%)
  starting transfers between devices  7.36 us (5%)
  other arithmetic  2.96 us (2%)
    all_to_all x1, waiting for transfers between devices, gather_turned(): lax.all_to_all(jnp.stack([both] * lax.axis_size(axis)), axis, 0, 0)  41.7 us
    psum x4, blocking collectives, over_axes(): return functools.reduce(lax.psum, axes, value)  38 us
    all_to_all x1, blocking collectives, sum_at_owner(): lax.all_to_all(pieces, axis, split_axis=0, concat_axis=0, tiled=True)  18 us
    unnamed x31, local copies, waits for them, and re-layouts  10.5 us
    dot_general x1, matrix products, on_device(): jnp.dot(normed_input, bases[1], preferred_element_type=jnp.float32)  6.11 us
    all_to_all x1, starting transfers between devices, gather_turned(): lax.all_to_all(jnp.stack([both] * lax.axis_size(axis)), axis, 0, 0)  3.74 us
    all_to_all x1, starting transfers between devices, sent_to_all(): return lax.all_to_all(copies, axis, split_axis=0, concat_axis=0, tiled=True)  3.61 us
    transpose x1, local copies, waits for them, and re-layouts, gather_turned(): finished.append(jnp.moveaxis(piece, 0, dim))  3.41 us
  transfers between devices with their start and end apart: 2, of which 1 were waited for; matrix products, arithmetic and copies ran while one was open for 5% of the time, Pallas kernels for 0%

profile of v1, /device:TPU:0, one launch (start us, length us, event | category | flops | bytes accessed | tf_op | source)
XLA Modules:
  0.0 145.8 jit_solution(774191283561381405)
XLA Ops:
  0.7 6.1 %convolution_bitcast_fusion.1 = f32[2048,1,256]{2,0,1:T(8,128)S(1)} fusion(bf16[2048,2048]{1,0:T(8,128)(2,1)} %param.11, bf16[3,2048,256]{2,1,0:T(8,128)(2,1)} %param.19), kind=kOutput, calls=%fused_computation.6 | convolution fusion | flops 2147483648 | bytes 11534336 | tf_op jit(solution)/shard_map/dot_general | solution.py:88
  7.7 2.5 %convolution_bitcast_fusion.2 = f32[2048,1,256]{2,0,1:T(8,128)S(1)} fusion(bf16[2048,2048]{1,0:T(8,128)(2,1)S(1)} %copy-done.6, bf16[3,2048,256]{2,1,0:T(8,128)(2,1)S(1)} %copy-done.3), kind=kOutput, calls=%fused_computation.7 | convolution fusion | flops 2147483648 | bytes 11534336 | tf_op jit(solution)/shard_map/dot_general | solution.py:87
  10.3 2.3 %convolution_bitcast_fusion = f32[2048,1,256]{2,0,1:T(8,128)S(1)} fusion(bf16[2048,2048]{1,0:T(8,128)(2,1)S(1)} %bitcast.57, bf16[3,2048,256]{2,1,0:T(8,128)(2,1)S(1)} %copy-done.3), kind=kOutput, calls=%fused_computation.5 | convolution fusion | flops 2147483648 | bytes 11534336 | tf_op jit(solution)/shard_map/dot_general | solution.py:89
  14.5 1.4 fusion.1
  16.0 1.3 fusion.5
  17.3 18.0 %all_to_all.15 = bf16[16,16,3,256]{3,1,2,0:T(8,128)(2,1)S(1)} all-to-all(bf16[16,16,3,256]{3,1,2,0:T(8,128)(2,1)S(1)} %copy.61), channel_id=1, replica_groups=mesh['fs_0'=4,'fs_1'=4,'tp_0'=4,'tp_1'=2] {'fs_0','fs_1'}, dimensions={0} | all-to-all | bytes 786432 | tf_op jit(solution)/shard_map/all_to_all | solution.py:20
  36.1 1.0 broadcast_in_dim.4
  37.1 3.6 %all-to-all-start.1 = ((f32[16,16,3,256]{3,1,2,0:T(8,128)}), f32[16,16,3,256]{3,1,2,0:T(8,128)S(1)}, u32[]{:S(2)}, u32[]{:S(2)}) async-start(f32[16,16,3,256]{3,1,2,0:T(8,128)} %broadcast_in_dim.4), calls=%async_computation.1 | async-start | bytes 1572864 | tf_op jit(solution)/shard_map/all_to_all | solution.py:32
  40.7 14.1 %psum.28 = f32[3]{0:T(128)S(1)} all-reduce(f32[3]{0:T(128)S(1)} %get-tuple-element.62), channel_id=1, replica_groups=mesh['fs_0'=4,'fs_1'=4,'tp_0'=4,'tp_1'=2] {'fs_0'}, use_global_device_ids=true, to_apply=%region_2.0 | all-reduce | flops 3 | bytes 24 | tf_op jit(solution)/shard_map/psum | solution.py:40
  54.8 10.5 %psum.29 = f32[3]{0:T(128)S(1)} all-reduce(f32[3]{0:T(128)S(1)} %psum.28), channel_id=1, replica_groups=mesh['fs_0'=4,'fs_1'=4,'tp_0'=4,'tp_1'=2] {'fs_1'}, use_global_device_ids=true, to_apply=%region_3.0 | all-reduce | flops 3 | bytes 24 | tf_op jit(solution)/shard_map/psum | solution.py:40
  65.5 10.8 %psum.30 = f32[3]{0:T(128)S(1)} all-reduce(f32[3]{0:T(128)S(1)} %psum.29), channel_id=1, replica_groups=mesh['fs_0'=4,'fs_1'=4,'tp_0'=4,'tp_1'=2] {'tp_0'}, use_global_device_ids=true, to_apply=%region_4.0 | all-reduce | flops 3 | bytes 24 | tf_op jit(solution)/shard_map/psum | solution.py:40
  76.2 2.6 %psum.31 = f32[3]{0:T(128)S(1)} all-reduce(f32[3]{0:T(128)S(1)} %psum.30), channel_id=1, replica_groups=mesh['fs_0'=4,'fs_1'=4,'tp_0'=4,'tp_1'=2] {'tp_1'}, use_global_device_ids=true, to_apply=%region_5.0 | all-reduce | flops 3 | bytes 24 | tf_op jit(solution)/shard_map/psum | solution.py:40
  79.1 1.2 fusion.16
  80.3 1.2 fusion.7
  83.1 2.3 %stack.51 = bf16[16,128,768]{1,2,0:T(8,128)(2,1)} broadcast(bf16[128,768]{0,1:T(8,128)(2,1)S(1)} %pad_maximum_fusion.10), dimensions={1,2} | broadcast | bytes 3342336 | tf_op jit(solution)/shard_map/stack | solution.py:48
  85.3 3.7 %all-to-all-start.2 = ((bf16[16,128,768]{1,2,0:T(8,128)(2,1)}), bf16[16,128,768]{1,2,0:T(8,128)(2,1)S(1)}, u32[]{:S(2)}, u32[]{:S(2)}) async-start(bf16[16,128,768]{1,2,0:T(8,128)(2,1)} %stack.51), calls=%async_computation.2 | async-start | bytes 6291456 | tf_op jit(solution)/shard_map/all_to_all | solution.py:48
  89.1 1.7 %copy.68 = f32[128,256]{1,0:T(8,128)} copy(f32[128,256]{0,1:T(8,128)} %get-tuple-element.72) | data formatting | bytes 262144
  90.7 1.7 %copy.69 = f32[128,256]{1,0:T(8,128)} copy(f32[128,256]{0,1:T(8,128)} %get-tuple-element.58) | data formatting | bytes 262144
  93.1 1.7 %copy.71 = f32[128,256]{1,0:T(8,128)} copy(f32[128,256]{0,1:T(8,128)} %get-tuple-element.70) | data formatting | bytes 262144
  94.8 1.7 %copy.72 = f32[128,256]{1,0:T(8,128)} copy(f32[128,256]{0,1:T(8,128)} %get-tuple-element.69) | data formatting | bytes 262144
  96.4 41.7 %all-to-all-done.2 = bf16[16,128,768]{1,2,0:T(8,128)(2,1)S(1)} async-done(((bf16[16,128,768]{1,2,0:T(8,128)(2,1)}), bf16[16,128,768]{1,2,0:T(8,128)(2,1)S(1)}, u32[]{:S(2)}, u32[]{:S(2)}) %all-to-all-start.2) | async-done | bytes 3145760 | tf_op jit(solution)/shard_map/all_to_all | solution.py:48
  138.1 2.8 %copy.67 = bf16[16,128,768]{2,1,0:T(8,128)(2,1)} copy(bf16[16,128,768]{1,2,0:T(8,128)(2,1)S(1)} %all-to-all-done.2) | data formatting | bytes 6291456 | tf_op jit(solution)/shard_map/all_to_all | solution.py:48
  140.9 3.4 %slice_bitcast_fusion = (bf16[256,2048]{0,1:T(8,128)(2,1)S(1)}, bf16[2048,256]{1,0:T(8,128)(2,1)}, bf16[2048,256]{1,0:T(8,128)(2,1)}) fusion(bf16[2048,768]{1,0:T(8,128)(2,1)} %bitcast.54), kind=kLoop, calls=%fused_computation.15 | loop fusion | bytes 6291456 | tf_op jit(solution)/shard_map/transpose | solution.py:55
  144.3 1.4 copy.70
  (40 shorter events, 6.2 us)
Async XLA Ops:
  0.6 6.2 %copy-start.3 = (bf16[3,2048,256]{2,1,0:T(8,128)(2,1)S(1)}, bf16[3,2048,256]{2,1,0:T(8,128)(2,1)}, u32[]{:S(2)}) copy-start(bf16[3,2048,256]{2,1,0:T(8,128)(2,1)} %param.19) | copy-start | bytes 9437188
  0.7 7.0 %copy-start.6 = (bf16[2048,2048]{1,0:T(8,128)(2,1)S(1)}, bf16[2048,2048]{1,0:T(8,128)(2,1)}, u32[]{:S(2)}) copy-start(bf16[2048,2048]{1,0:T(8,128)(2,1)} %param.11) | copy-start | bytes 25165828
  0.7 9.5 %slice-start = ((s8[8388608]{0:T(1024)(128)(4,1)}), s8[4194304]{0:T(1024)(128)(4,1)S(1)}, s32[]{:S(2)}) async-start(s8[8388608]{0:T(1024)(128)(4,1)} %bitcast.56), calls=%async_computation.3 | async-start | bytes 8388608
  7.7 2.6 %slice-start.1 = ((s8[8388608]{0:T(1024)(128)(4,1)}), s8[4194304]{0:T(1024)(128)(4,1)S(1)}, s32[]{:S(2)}) async-start(s8[8388608]{0:T(1024)(128)(4,1)} %bitcast.56), calls=%async_computation.4 | async-start | bytes 8388608
  12.6 1.2 copy-start.7
  12.7 1.5 %copy-start.8 = (bf16[2048,256]{1,0:T(8,128)(2,1)S(1)}, bf16[2048,256]{1,0:T(8,128)(2,1)}, u32[]{:S(2)}) copy-start(bf16[2048,256]{1,0:T(8,128)(2,1)} %param.13) | copy-start | bytes 3145732
  12.7 1.8 %copy-start.9 = (bf16[2048,256]{1,0:T(8,128)(2,1)S(1)}, bf16[2048,256]{1,0:T(8,128)(2,1)}, u32[]{:S(2)}) copy-start(bf16[2048,256]{1,0:T(8,128)(2,1)} %param.12) | copy-start | bytes 3145732
  15.9 19.5 %copy-start.4 = (f32[16,3,256]{2,0,1:T(8,128)S(1)}, f32[16,3,256]{2,0,1:T(8,128)}, u32[]{:S(2)}) copy-start(f32[16,3,256]{2,0,1:T(8,128)} %param.21) | copy-start | bytes 147460
  16.0 19.5 %copy-start.5 = (f32[16,3,256]{2,0,1:T(8,128)S(1)}, f32[16,3,256]{2,0,1:T(8,128)}, u32[]{:S(2)}) copy-start(f32[16,3,256]{2,0,1:T(8,128)} %param.20) | copy-start | bytes 147460
  17.3 37.5 %copy-start = (f32[128,256]{1,0:T(8,128)S(1)}, f32[128,256]{1,0:T(8,128)}, u32[]{:S(2)}) copy-start(f32[128,256]{1,0:T(8,128)} %param.16) | copy-start | bytes 393220
  17.3 48.1 %copy-start.1 = (f32[128,256]{1,0:T(8,128)S(1)}, f32[128,256]{1,0:T(8,128)}, u32[]{:S(2)}) copy-start(f32[128,256]{1,0:T(8,128)} %param.17) | copy-start | bytes 393220
  37.1 41.8 %all-to-all-start.1 = ((f32[16,16,3,256]{3,1,2,0:T(8,128)}), f32[16,16,3,256]{3,1,2,0:T(8,128)S(1)}, u32[]{:S(2)}, u32[]{:S(2)}) async-start(f32[16,16,3,256]{3,1,2,0:T(8,128)} %broadcast_in_dim.4), calls=%async_computation.1 | async-start | bytes 1572864 | tf_op jit(solution)/shard_map/all_to_all | solution.py:32
  78.8 2.7 %copy-start.2 = (f32[256,128]{1,0:T(8,128)S(1)}, f32[256,128]{1,0:T(8,128)}, u32[]{:S(2)}) copy-start(f32[256,128]{1,0:T(8,128)} %param.18) | copy-start | bytes 393220
  85.3 52.8 %all-to-all-start.2 = ((bf16[16,128,768]{1,2,0:T(8,128)(2,1)}), bf16[16,128,768]{1,2,0:T(8,128)(2,1)S(1)}, u32[]{:S(2)}, u32[]{:S(2)}) async-start(bf16[16,128,768]{1,2,0:T(8,128)(2,1)} %stack.51), calls=%async_computation.2 | async-start | bytes 6291456 | tf_op jit(solution)/shard_map/all_to_all | solution.py:48
